TPU v7x, 32 devices: a whole 2x2x4 slice. The times are simulated.
32 devices in a mesh: grp: 2 (over y), dp: 2 (over x), kv: 4 (over z), tp: 2 (over core).
Axes of the slice: x: 2, y: 2, z: 4, core: 2. Of those that a mesh axis runs over, the one named last changes fastest.
Arguments:
- tokens: bfloat16 [32, 2048], P(('grp', 'dp'), 'kv'), parts along dimension 0, may hold values from -110 to 110
- attend_gain: float32 [2048], P('kv'), may hold values from 0.1 to 1.9
- query_weight: bfloat16 [2048, 2048], P('kv', 'tp'), may hold values from -0.125 to 0.125
- cache_keys: bfloat16 [32, 1536, 2, 128], P(('grp', 'dp'), 'kv', 'tp'), parts along dimension 0, may hold values from -1600 to 1600
- cache_values: bfloat16 [32, 1536, 2, 128], P(('grp', 'dp'), 'kv', 'tp'), parts along dimension 0, may hold values from -6 to 6
- head_lambda: float32 [16], P('tp'), may hold values from 0.3 to 0.8
- head_gain: float32 [128], replicated, may hold values from 0.1 to 1.9
- output_weight: bfloat16 [2048, 2048], P('tp', 'kv'), may hold values from -0.125 to 0.125
- mixer_gain: float32 [2048], P('kv'), may hold values from 0.1 to 1.9
- gate_weight: bfloat16 [2048, 5632], P('kv', 'tp'), may hold values from -0.125 to 0.125
- up_weight: bfloat16 [2048, 5632], P('kv', 'tp'), may hold values from -0.125 to 0.125
- down_weight: bfloat16 [5632, 2048], P('tp', 'kv'), may hold values from -0.078125 to 0.078125
Outputs:
- layer_out: bfloat16 [32, 2048], P(('grp', 'dp'), 'kv'), parts along dimension 0
There are 2 independent parts, one for each index of `grp`. A program takes and returns all parts, laid end to end along the dimension named above; an argument that names none is the same for every part. Nothing has to cross between parts.
All inputs are finite; a program needn't handle non-finite values.
Results may differ from a plain program's by a relative error of at most 0.025.
Values may be sent and summed in bfloat16 or wider, within the bound.
A program may use at most 64 MiB of HBM per device.

v0:
```python
import jax
import jax.numpy as jnp
from jax import lax
from jax.sharding import PartitionSpec as P

D = 2048
HD = 64
VD = 128


ROPE_BASE = 500000.0
EPSILON = 1e-06
KEEP_SCALE = 0.8


def merged(array, axis, join):
    gathered = jax.tree.map(
        lambda a, kind: lax.all_gather(a.astype(kind), axis),
        array,
        (jnp.bfloat16, jnp.bfloat16, jnp.bfloat16),
    )

    def take(source):
        return jax.tree.map(
            lambda a, own: lax.dynamic_index_in_dim(a, source, 0, False).astype(own.dtype),
            gathered,
            array,
        )

    return lax.fori_loop(
        1, lax.axis_size(axis), lambda source, state: join(state, take(source)), take(0)
    )


def rotate(query, position):
    half_dim = query.shape[-1] // 2
    frequency = ROPE_BASE ** (-jnp.arange(half_dim, dtype=jnp.float32) * 2.0 / query.shape[-1])
    angles = position * frequency
    cosine_part = jnp.cos(angles)
    sine_part = jnp.sin(angles)
    first_half = query[..., :half_dim]
    second_half = query[..., half_dim:]
    return jnp.concatenate(
        [
            first_half * cosine_part - second_half * sine_part,
            second_half * cosine_part + first_half * sine_part,
        ],
        axis=-1,
    )


def combine(left_part, right_part):
    left_max, left_total, left_sum = left_part
    right_max, right_total, right_sum = right_part
    joint_max = jnp.maximum(left_max, right_max)
    left_factor = jnp.exp(left_max - joint_max)
    right_factor = jnp.exp(right_max - joint_max)
    return (
        joint_max,
        left_total * left_factor + right_total * right_factor,
        left_sum * left_factor[..., None] + right_sum * right_factor[..., None],
    )


def on_device(
    tokens,
    attend_gain,
    query_weight,
    cache_keys,
    cache_values,
    head_lambda,
    head_gain,
    output_weight,
    mixer_gain,
    gate_weight,
    up_weight,
    down_weight,
):
    seq_rows = tokens.shape[0]
    heads_here = head_lambda.shape[0]
    kv_local = cache_keys.shape[2]
    group_size = heads_here // kv_local
    positions = cache_keys.shape[1]
    context = positions * lax.axis_size("kv")
    tok_float = tokens.astype(jnp.float32)
    scaled = (tok_float * attend_gain).astype(jnp.bfloat16)
    partial_query = jnp.dot(scaled, query_weight, preferred_element_type=jnp.float32)
    query_sum, squares = (
        lax.psum(partial_query.astype(jnp.bfloat16), "kv").astype(jnp.float32),
        lax.psum(jnp.sum(tok_float * tok_float, axis=1).astype(jnp.bfloat16), "kv").astype(
            jnp.float32
        ),
    )
    attend_scale = lax.rsqrt(squares / D + EPSILON)[:, None]
    query = (attend_scale * query_sum).reshape(seq_rows, kv_local, group_size, 2, HD)
    query = rotate(query, jnp.asarray(context, jnp.float32)).astype(jnp.bfloat16)
    key_block = cache_keys.reshape(seq_rows, positions, kv_local, 2, HD)
    scores = jnp.einsum(
        "skgcd,spkcd->skgcp", query, key_block, preferred_element_type=jnp.float32
    ) * HD ** (-0.5)
    row_max = jnp.max(scores, axis=-1)
    exponent = jnp.exp(scores - row_max[..., None])
    row_total = jnp.sum(exponent, axis=-1)
    weighted = jnp.einsum(
        "skgcp,spke->skgce",
        exponent.astype(jnp.bfloat16),
        cache_values,
        preferred_element_type=jnp.float32,
    )
    row_max, row_total, weighted = merged((row_max, row_total, weighted), "kv", combine)
    averaged = weighted / row_total[..., None]
    lambda_grid = head_lambda.reshape(kv_local, group_size)[None, :, :, None]
    difference = averaged[:, :, :, 0] - lambda_grid * averaged[:, :, :, 1]
    normed = difference * lax.rsqrt(
        jnp.mean(difference * difference, axis=-1, keepdims=True) + EPSILON
    )
    heads_out = (
        (normed * head_gain * KEEP_SCALE).astype(jnp.bfloat16).reshape(seq_rows, heads_here * VD)
    )
    attended = lax.psum(
        jnp.dot(heads_out, output_weight, preferred_element_type=jnp.float32).astype(jnp.bfloat16),
        "tp",
    ).astype(jnp.float32)
    middle = (tok_float + attended).astype(jnp.bfloat16)
    mid_float = middle.astype(jnp.float32)
    mixer_in = (mid_float * mixer_gain).astype(jnp.bfloat16)
    gate_part = jnp.dot(mixer_in, gate_weight, preferred_element_type=jnp.float32)
    up_part = jnp.dot(mixer_in, up_weight, preferred_element_type=jnp.float32)
    mid_squares = jnp.sum(mid_float * mid_float, axis=1)
    gate_sum, up_sum, total_squares = (
        lax.psum(gate_part.astype(jnp.bfloat16), "kv").astype(jnp.float32),
        lax.psum(up_part.astype(jnp.bfloat16), "kv").astype(jnp.float32),
        lax.psum(mid_squares.astype(jnp.bfloat16), "kv").astype(jnp.float32),
    )
    mixer_scale = lax.rsqrt(total_squares / D + EPSILON)[:, None]
    hidden = (jax.nn.silu(mixer_scale * gate_sum) * (mixer_scale * up_sum)).astype(jnp.bfloat16)
    projected = jnp.dot(hidden, down_weight, preferred_element_type=jnp.float32)
    mixed = lax.psum(projected.astype(jnp.bfloat16), "tp").astype(jnp.float32)
    return (mid_float + mixed).astype(jnp.bfloat16)


def solution(mesh):
    return jax.shard_map(
        on_device,
        mesh=mesh,
        in_specs=(
            P(("grp", "dp"), "kv"),
            P("kv"),
            P("kv", "tp"),
            P(("grp", "dp"), "kv", "tp", None),
            P(("grp", "dp"), "kv", "tp", None),
            P("tp"),
            P(),
            P("tp", "kv"),
            P("kv"),
            P("kv", "tp"),
            P("kv", "tp"),
            P("tp", "kv"),
        ),
        out_specs=P(("grp", "dp"), "kv"),
        check_vma=False,
    )
```

profile of v0, /device:TPU:0, one launch (start us, length us, event | category | flops | bytes accessed | tf_op | source)
XLA Modules:
  0.0 131.3 jit_solution(4138860294663475520)
XLA Ops:
  6.5 0.0 copy-start
  6.5 0.0 all-reduce.4.cloned.1.call-start
  6.6 1.0 fusion.25
  7.6 1.5 %convolution_convert_fusion.3 = bf16[8,1024]{1,0:T(8,128)(2,1)S(1)} fusion(bf16[512,1024]{1,0:T(8,128)(2,1)} %param.16, bf16[8,512]{1,0:T(8,128)(2,1)} %param.14, f32[512]{0:T(512)} %param.15), kind=kOutput, calls=%fused_computation.21 | convolution fusion | flops 8409088 | bytes 1075200 | tf_op jit(solution)/shard_map/dot_general | solution.py:87
  9.1 20.7 %all-reduce.1 = (bf16[8,1024]{1,0:T(8,128)(2,1)S(1)}, bf16[8]{0:T(256)(128)(2,1)S(1)}) all-reduce(bf16[8,1024]{1,0:T(8,128)(2,1)S(1)} %convolution_convert_fusion.3, bf16[8]{0:T(256)(128)(2,1)S(1)} %fusion.25), channel_id=1, replica_groups=mesh['grp'=2,'dp'=2,'kv'=4,'tp'=2] {'kv'}, use_global_device_ids=true, to_apply=%region_2.0 | all-reduce | flops 8200 | bytes 32800 | tf_op jit(solution)/shard_map/psum | solution.py:89
  29.8 0.1 convert_multiply_fusion.2
  29.8 0.1 reshape.262
  30.0 0.1 fusion.49
  30.1 2.3 %copy.55 = bf16[8,384,1,128]{1,3,0,2:T(8,128)(2,1)} copy(bf16[8,384,1,128]{3,1,2,0:T(8,128)(2,1)} %param.17) | data formatting | bytes 1572864 | tf_op args[3]
  32.4 0.0 copy-start.4
  32.4 0.0 copy-start.5
  32.4 1.5 %fusion.50 = (f32[8,8,2]{1,2,0:T(2,128)S(1)}, f32[8,1,8,2,384]{4,2,3,0,1:T(8,128)S(1)}) fusion(bf16[8,384,2,64]{1,3,2,0:T(8,128)(2,1)} %bitcast.108, bf16[8,8,2,32]{3,1,2,0:T(8,128)(2,1)S(1)} %get-tuple-element.240, bf16[8,8,2,32]{3,1,2,0:T(8,128)(2,1)S(1)} %get-tuple-element.239), kind=kOutput, calls=%fused_computation.86 | convolution fusion | flops 6422400 | bytes 999936 | tf_op jit(solution)/shard_map/skgcd,spkcd->skgcp/dot_general | solution.py:98
  34.0 0.2 fusion.8
  34.2 0.0 copy-start.2
  34.2 0.0 copy-start.3
  34.2 1.5 %convolution_convert_fusion.2 = bf16[8,8,2,128]{3,1,2,0:T(8,128)(2,1)S(1)} fusion(bf16[8,384,1,128]{3,1,2,0:T(8,128)(2,1)} %param.18, f32[8,1,8,2,384]{4,2,3,0,1:T(8,128)S(1)} %get-tuple-element.247, f32[8,8,2]{1,2,0:T(2,128)S(1)} %get-tuple-element.246), kind=kOutput, calls=%fused_computation.20 | convolution fusion | flops 12697600 | bytes 1016320 | tf_op jit(solution)/shard_map/skgcp,spke->skgce/dot_general | solution.py:104
  35.7 13.4 %all-gather.2 = bf16[32,8,2,128]{3,1,2,0:T(8,128)(2,1)S(1)} all-gather(bf16[8,8,2,128]{3,1,2,0:T(8,128)(2,1)S(1)} %convolution_convert_fusion.2), channel_id=4, replica_groups=mesh['grp'=2,'dp'=2,'kv'=4,'tp'=2] {'kv'}, dimensions={0}, use_global_device_ids=true | all-gather | bytes 163840 | tf_op jit(solution)/shard_map/all_gather | solution.py:18
  49.1 13.2 %all-gather.1 = bf16[32,8,2]{1,2,0:T(2,128)(2,1)S(1)} all-gather(bf16[8,8,2]{1,2,0:T(2,128)(2,1)S(1)} %fusion.8), channel_id=3, replica_groups=mesh['grp'=2,'dp'=2,'kv'=4,'tp'=2] {'kv'}, dimensions={0}, use_global_device_ids=true | all-gather | bytes 1280 | tf_op jit(solution)/shard_map/all_gather | solution.py:18
  62.3 13.2 %all-gather = bf16[32,8,2]{1,2,0:T(2,128)(2,1)S(1)} all-gather(bf16[8,8,2]{1,2,0:T(2,128)(2,1)S(1)} %convert_element_type.221), channel_id=2, replica_groups=mesh['grp'=2,'dp'=2,'kv'=4,'tp'=2] {'kv'}, dimensions={0}, use_global_device_ids=true | all-gather | bytes 1280 | tf_op jit(solution)/shard_map/all_gather | solution.py:18
  75.6 2.3 %while.19 = (s32[]{:T(128)}, f32[8,1,8,2]{2,0,3,1:T(8,128)S(1)}, f32[8,1,8,2]{2,0,3,1:T(8,128)S(1)}, f32[8,1,8,2,128]{4,3,2,1,0:T(2,128)S(1)}, bf16[4,8,1,8,2]{3...) while((s32[]{:T(128)}, f32[8,1,8,2]{2,0,3,1:T(8,128)S(1)}, ...), condition=%wide.region_6.7_spmd, body=%wide.region_5.6_spmd.sunk | while | flops 66821 | bytes 239511 | solution.py:30
  75.6 0.1 copy.118
  75.8 0.1 copy.119
  75.9 0.4 fusion.62
  76.4 0.1 copy.118
  76.5 0.1 copy.119
  76.6 0.4 fusion.62
  77.2 0.1 copy.118
  77.3 0.1 copy.119
  77.4 0.4 fusion.62
  77.8 0.1 copy.62
  78.0 0.1 broadcast_divide_fusion
  78.1 0.1 fusion.48
  78.2 0.0 copy-done.4
  78.2 0.2 multiply_reduce_fusion
  78.4 0.1 copy.64
  78.5 0.0 copy-done.5
  78.5 0.1 broadcast_bitcast_fusion
  78.6 1.5 %convolution_convert_fusion.5 = bf16[8,512]{1,0:T(8,128)(2,1)S(1)} fusion(bf16[1024,512]{1,0:T(8,128)(2,1)} %param.21, f32[1,8,8,128]{3,2,1,0:T(8,128)S(1)} %bitcast.113, f32[1,8,8,128]{3,2,1,0:T(8,128)S(1)} %bitcast.112, f32[1024]{0:T(1024)S(1)} %get-tuple-element.250, f32[8,8]{0,1:T(8,128)S(1)} %copy.64, f32[1024]{0:T(1024)S(1)} %get-tuple-element.251), kind=kOutput, calls=%fused_computation.23 | convolution fusion | flops 8441856 | bytes 1130752 | tf_op jit(solution)/shard_map/dot_general | solution.py:121
  80.1 2.5 %psum.51 = bf16[8,512]{1,0:T(8,128)(2,1)S(1)} all-reduce(bf16[8,512]{1,0:T(8,128)(2,1)S(1)} %convolution_convert_fusion.5), channel_id=1, replica_groups=mesh['grp'=2,'dp'=2,'kv'=4,'tp'=2] {'tp'}, use_global_device_ids=true, to_apply=%region_8.9 | all-reduce | flops 4096 | bytes 16384 | tf_op jit(solution)/shard_map/psum | solution.py:120
  82.5 0.0 copy-done.2
  82.5 0.0 copy-start.1
  82.6 0.6 fusion.28
  83.2 0.0 copy-done
  83.2 0.0 copy-done.3
  83.2 1.1 convolution_convert_fusion
  84.3 0.1 copy-done.1
  84.4 1.1 convolution_convert_fusion.1
  85.5 0.0 all-reduce.4.cloned.1.call-update
  85.5 32.8 %all-reduce.4.cloned.1.call-done = (bf16[8,2816]{1,0:T(8,128)(2,1)}, bf16[8,2816]{1,0:T(8,128)(2,1)}, bf16[8]{0:T(256)(128)(2,1)}) async-done(((bf16[8,2816]{1,0:T(8,128)(2,1)}, bf16[8,2816]{1,0:T(8,128)(2,1)}, bf16[8]{0:T(256)(128)(2,1)}), (bf16[8,2816]{1,0:T(8,128)(2,1)}, bf16[8,2816]{1,0:T(8,128)(2,1)}, bf16[8]{0:T(256)(128)(2,1)})) %all-reduce.4.cloned.1.call-update) | async-done | bytes 90144 | tf_op jit(solution)/shard_map/psum | solution.py:132
  118.3 0.7 add_rsqrt_fusion.1
  118.9 2.4 %convolution_convert_fusion.4 = bf16[8,512]{1,0:T(8,128)(2,1)S(1)} fusion(bf16[2816,512]{1,0:T(8,128)(2,1)} %param.25, bf16[8,2816]{1,0:T(8,128)(2,1)} %get-tuple-element.226, bf16[8,2816]{1,0:T(8,128)(2,1)} %get-tuple-element.227, f32[8]{0:T(128)S(1)} %add_rsqrt_fusion.1), kind=kOutput, calls=%fused_computation.22 | convolution fusion | flops 23298048 | bytes 2981920 | tf_op jit(solution)/shard_map/dot_general | solution.py:137
  121.3 2.5 %psum.55 = bf16[8,512]{1,0:T(8,128)(2,1)S(1)} all-reduce(bf16[8,512]{1,0:T(8,128)(2,1)S(1)} %convolution_convert_fusion.4), channel_id=1, replica_groups=mesh['grp'=2,'dp'=2,'kv'=4,'tp'=2] {'tp'}, use_global_device_ids=true, to_apply=%region_13.14 | all-reduce | flops 4096 | bytes 16384 | tf_op jit(solution)/shard_map/psum | solution.py:138
  123.8 0.6 fusion.30
  (26 shorter events, 0.3 us)
Async XLA Ops:
  6.5 76.7 %copy-start = (bf16[512,2816]{1,0:T(8,128)(2,1)S(1)}, bf16[512,2816]{1,0:T(8,128)(2,1)}, u32[]{:S(2)}) copy-start(bf16[512,2816]{1,0:T(8,128)(2,1)} %param.24) | copy-start | bytes 8650756
  6.5 111.7 %all-reduce.4.cloned.1.call-start = ((), (), s32[]{:S(2)}) async-start(), calls=%async_computation | async-start | bytes 181248 | tf_op jit(solution)/shard_map/psum | solution.py:132
  32.4 45.8 %copy-start.4 = (f32[8]{0:T(128)S(1)}, f32[8]{0:T(128)}, u32[]{:S(2)}) copy-start(f32[8]{0:T(128)} %param.19) | copy-start | bytes 100
  32.4 46.1 %copy-start.5 = (f32[128]{0:T(128)S(1)}, f32[128]{0:T(128)}, u32[]{:S(2)}) copy-start(f32[128]{0:T(128)} %param.20) | copy-start | bytes 1540
  34.2 48.4 %copy-start.2 = (bf16[8,512]{1,0:T(8,128)(2,1)S(1)}, bf16[8,512]{1,0:T(8,128)(2,1)}, u32[]{:S(2)}) copy-start(bf16[8,512]{1,0:T(8,128)(2,1)} %param.14) | copy-start | bytes 24580
  34.2 49.0 %copy-start.3 = (f32[512]{0:T(512)S(1)}, f32[512]{0:T(512)}, u32[]{:S(2)}) copy-start(f32[512]{0:T(512)} %param.22) | copy-start | bytes 6148
  82.5 1.8 %copy-start.1 = (bf16[512,2816]{1,0:T(8,128)(2,1)S(1)}, bf16[512,2816]{1,0:T(8,128)(2,1)}, u32[]{:S(2)}) copy-start(bf16[512,2816]{1,0:T(8,128)(2,1)} %param.23) | copy-start | bytes 8650756
Sparse Core Ops, SparseCore 0:
  85.6 32.6 all-reduce.3
where the time goes:
time: 132 us; the launch traced here: 131 us
  blocking collectives  65.5 us (50%)
  waiting for transfers between devices  32.8 us (25%)
  between operations  13.5 us (10%)
  matrix products  10.6 us (8%)
  other arithmetic  4.88 us (4%)
  local copies, waits for them, and re-layouts  3.83 us (3%)
    all_gather x3, blocking collectives, merged(): lax.all_gather(a.astype(kind), axis)  39.8 us
    psum x1, waiting for transfers between devices, on_device(): lax.psum(up_part.astype(jnp.bfloat16), 'kv').astype(jnp.float32)  32.8 us
    psum x1, blocking collectives, on_device(): lax.psum(partial_query.astype(jnp.bfloat16), 'kv').astype(jnp.float32)  20.7 us
  transfers between devices with their start and end apart: 1, of which 1 were waited for; matrix products, arithmetic and copies ran while one was open for 0% of the time, Pallas kernels for 0%

commit v1 on v0

v1 whole, which is shorter than its diff:
```python
import functools

import jax
import jax.numpy as jnp
import numpy as np
from jax import lax
from jax.experimental import pallas as pl
from jax.experimental.pallas import tpu as pltpu
from jax.sharding import PartitionSpec as P

HD = 64
ROPE_BASE = 500000.0
EPSILON = 1e-06
KEEP_SCALE = 0.8
LANES = 128
B_PARTS = 2
F32 = jnp.float32
BF16 = jnp.bfloat16


def high_low(column):
    high = column.astype(BF16).astype(F32)
    low = column - high
    lane = lax.broadcasted_iota(jnp.int32, (column.shape[0], LANES), 1)
    return jnp.where(lane < LANES // 2, high, low).astype(BF16)


def from_high_low(tile):
    tile = tile.astype(F32)
    return tile[:, 0:1] + tile[:, LANES // 2 : LANES // 2 + 1]


def kernel(
    n_kv,
    n_tp,
    n_pieces,
    widths,
    features,
    tok_hbm,
    again_hbm,
    wq_hbm,
    key_hbm,
    val_hbm,
    lam_hbm,
    hgain_hbm,
    wo_hbm,
    mgain_hbm,
    wg_hbm,
    wu_hbm,
    wd_hbm,
    rope_hbm,
    out_ref,
    tok,
    again,
    wq,
    keys,
    vals,
    lam,
    hgain,
    wo,
    mgain,
    wg,
    wu,
    wd,
    rope,
    a_send,
    a_recv,
    b_send,
    b_recv,
    s_send,
    s_recv,
    c_send,
    c_recv,
    d_sends,
    d_recvs,
    e_alls,
    f_send,
    f_recv,
    query_rows,
    head_rows,
    load_sem,
    kv_send,
    kv_recv,
    piece_send,
    tp_send,
    tp_recv,
):
    me = lax.axis_index("kv")
    core = lax.axis_index("tp")
    rows = tok.shape[0]
    heads = lam.shape[1]
    hidden_here = wg_hbm.shape[1]

    loads = []
    for index, (source, target) in enumerate(
        [
            (tok_hbm, tok),
            (again_hbm, again),
            (wq_hbm, wq),
            (rope_hbm, rope),
            (lam_hbm, lam),
            (hgain_hbm, hgain),
            (mgain_hbm, mgain),
            (key_hbm, keys),
            (val_hbm, vals),
            (wo_hbm, wo),
            (wg_hbm, wg),
            (wu_hbm, wu),
            (wd_hbm, wd),
        ]
    ):
        copy = pltpu.make_async_copy(source, target, load_sem.at[index])
        copy.start()
        loads.append(copy)

    barrier = pltpu.get_barrier_semaphore()
    for k in range(1, n_kv):
        pl.semaphore_signal(
            barrier,
            inc=1,
            device_id={"kv": lax.rem(me + k, n_kv)},
            device_id_type=pl.DeviceIdType.MESH,
        )
    for k in range(1, n_tp):
        pl.semaphore_signal(
            barrier,
            inc=1,
            device_id={"tp": lax.rem(core + k, n_tp)},
            device_id_type=pl.DeviceIdType.MESH,
        )

    pending = []
    half = max(n_kv // 2, 1)
    on_left = me < half

    def far_first(j):
        below, above = n_kv - 1 - j, j
        below = jnp.where(below > me, below, below - 1)
        above = jnp.where(above < me, above, above + 1)
        return jnp.where(on_left, below, above)

    peers = [far_first(j) for j in range(n_kv - 1)]

    def kv_copy(phase, source, target, slot_sent, slot_received, peer):
        return pltpu.make_async_remote_copy(
            src_ref=source,
            dst_ref=target,
            send_sem=kv_send.at[phase, slot_sent],
            recv_sem=kv_recv.at[phase, slot_received],
            device_id={"kv": peer},
            device_id_type=pl.DeviceIdType.MESH,
        )

    def to_all(phase, source, landing):
        for j, peer in enumerate(peers):
            copy = kv_copy(phase, source, landing(me), j, me, peer)
            copy.start()
            pending.append(copy)

    def from_kv(phase, landing, origin):
        kv_copy(phase, landing, landing, 0, origin, origin).wait_recv()

    def to_tp(phase, k, source, target):
        copy = pltpu.make_async_remote_copy(
            src_ref=source,
            dst_ref=target,
            send_sem=tp_send.at[phase, k - 1],
            recv_sem=tp_recv.at[phase, k - 1],
            device_id={"tp": lax.rem(core + k, n_tp)},
            device_id_type=pl.DeviceIdType.MESH,
        )
        copy.start()
        pending.append(copy)
        return copy

    for index in (0, 1, 2):
        loads[index].wait()
    tok_float = tok[...].astype(F32)
    scaled = (tok_float * again[...]).astype(BF16)
    query_part = jnp.dot(scaled, wq[...], preferred_element_type=F32)
    squares = jnp.sum(tok_float * tok_float, axis=1, keepdims=True)
    query_width = wq.shape[1]
    a_send[:, :query_width] = query_part.astype(BF16)
    a_send[:, query_width:] = high_low(squares)
    pl.semaphore_wait(barrier, n_kv - 1 + n_tp - 1)
    to_all(0, a_send, lambda slot: a_recv.at[slot])
    for index in (3, 4, 5, 6, 7):
        loads[index].wait()
    for peer in reversed(peers):
        from_kv(0, a_recv.at[peer], peer)
        query_part = query_part + a_recv[peer, :, :query_width].astype(F32)
        squares = squares + from_high_low(a_recv[peer, :, query_width:])
    query = query_part * lax.rsqrt(squares / features + EPSILON)

    lane = lax.broadcasted_iota(jnp.int32, (rows, LANES), 1)
    lower = lax.rem(lane, HD) < HD // 2
    cosine = rope[0:1, :]
    sine = rope[1:2, :]
    for h in range(heads):
        block = query[:, h * LANES : (h + 1) * LANES]
        partner = jnp.where(
            lower,
            pltpu.roll(block, LANES - HD // 2, 1),
            pltpu.roll(block, HD // 2, 1),
        )
        query_rows[h * rows : (h + 1) * rows, :] = block * cosine + partner * sine

    head_lane = lax.broadcasted_iota(jnp.int32, (heads, LANES), 1)
    scores = []
    for b in range(rows):
        turned = query_rows[pl.ds(b, heads, stride=rows), :]
        rounded = turned.astype(BF16).astype(F32) * HD ** (-0.5)
        both = jnp.concatenate(
            [
                jnp.where(head_lane < HD, rounded, 0.0),
                jnp.where(head_lane < HD, 0.0, rounded),
            ],
            axis=0,
        ).astype(BF16)
        scores.append(
            lax.dot_general(
                both, keys[b], (((1,), (1,)), ((), ())), preferred_element_type=F32
            )
        )
    loads[8].wait()
    count = 2 * heads
    all_rows = rows * count
    weighted, row_max, row_total = [], [], []
    for b in range(rows):
        top = jnp.max(scores[b], axis=1, keepdims=True)
        exponent = jnp.exp(scores[b] - top)
        row_max.append(top)
        row_total.append(jnp.sum(exponent, axis=1, keepdims=True))
        own = jnp.dot(exponent.astype(BF16), vals[b], preferred_element_type=F32)
        b_send[b * count : (b + 1) * count, :] = own.astype(BF16)
        weighted.append(own)
        if (b + 1) % (rows // B_PARTS) == 0:
            part = b // (rows // B_PARTS)
            span = pl.ds(part * (all_rows // B_PARTS), all_rows // B_PARTS)
            to_all(1 + part, b_send.at[span], lambda slot: b_recv.at[slot, span])
    diagonal = lax.broadcasted_iota(jnp.int32, (all_rows, all_rows), 0) == (
        lax.broadcasted_iota(jnp.int32, (all_rows, all_rows), 1)
    )

    def to_lanes(column):
        return jnp.sum(jnp.where(diagonal, column, 0.0), axis=0, keepdims=True)

    def to_rows(line):
        return jnp.sum(jnp.where(diagonal, line, 0.0), axis=1, keepdims=True)

    own_max = to_lanes(jnp.concatenate(row_max, axis=0))
    own_total = to_lanes(jnp.concatenate(row_total, axis=0))
    s_send[0:1, :] = own_max
    s_send[1:2, :] = own_total
    to_all(5, s_send, lambda slot: s_recv.at[slot])
    weighted = jnp.concatenate(weighted, axis=0)
    eye = lax.broadcasted_iota(jnp.int32, (heads, heads), 0) == (
        lax.broadcasted_iota(jnp.int32, (heads, heads), 1)
    )
    lam_column = jnp.sum(jnp.where(eye, lam[...], 0.0), axis=1, keepdims=True)
    for peer in reversed(peers):
        from_kv(5, s_recv.at[peer], peer)
    maxima = [own_max] + [s_recv[peer, 0:1, :] for peer in reversed(peers)]
    totals = [own_total] + [s_recv[peer, 1:2, :] for peer in reversed(peers)]
    joint = functools.reduce(jnp.maximum, maxima)
    factors = [jnp.exp(m - joint) for m in maxima]
    total = functools.reduce(jnp.add, [f * t for f, t in zip(factors, totals)])
    averaged = weighted * to_rows(factors[0] / total)
    shares = [to_rows(f / total) for f in factors[1:]]
    for share, peer in zip(shares, reversed(peers)):
        for part in range(B_PARTS):
            span = pl.ds(part * (all_rows // B_PARTS), all_rows // B_PARTS)
            from_kv(1 + part, b_recv.at[peer, span], peer)
        averaged = averaged + b_recv[peer].astype(F32) * share
    averaged = averaged.reshape(rows, 2, heads, LANES)
    difference = averaged[:, 0] - lam_column[None] * averaged[:, 1]
    normed = difference * lax.rsqrt(
        jnp.mean(difference * difference, axis=-1, keepdims=True) + EPSILON
    )
    normed = normed * (hgain[...] * KEEP_SCALE)[None]
    head_rows[...] = normed.reshape(rows * heads, LANES)
    heads_out = jnp.concatenate(
        [head_rows[pl.ds(h, rows, stride=heads), :] for h in range(heads)], axis=1
    ).astype(BF16)

    loads[9].wait()
    attended = jnp.dot(heads_out, wo[...], preferred_element_type=F32).astype(BF16)
    c_send[...] = attended
    copies = [to_tp(0, k, c_send, c_recv.at[k - 1]) for k in range(1, n_tp)]
    attended = attended.astype(F32)
    for index in (10, 11):
        loads[index].wait()
    for k, copy in enumerate(copies):
        copy.wait_recv()
        attended = attended + c_recv[k].astype(F32)
    mid_float = (tok_float + attended).astype(BF16).astype(F32)
    mixer_in = (mid_float * mgain[...]).astype(BF16)
    squares = jnp.sum(mid_float * mid_float, axis=1, keepdims=True)

    square_tile = high_low(squares)
    near = jnp.where(on_left, 0, n_pieces - 1)
    far = n_pieces - 1 - near
    first = (n_kv - n_pieces) // 2
    reduces = jnp.logical_and(me >= first, me < first + n_pieces)
    span = hidden_here // n_pieces
    starts = [sum(widths[:j]) for j in range(len(widths))]
    grids = list(zip(d_sends, d_recvs, e_alls, widths, starts))
    d_copies = []
    for piece in ([far] if n_pieces > 1 else []) + [near]:
        target = first + piece
        for j, (d_send, d_recv, _, width, start) in enumerate(grids):
            columns = pl.ds(pl.multiple_of(piece * span + start, LANES), width)
            gate = jnp.dot(mixer_in, wg[:, columns], preferred_element_type=F32)
            d_send[piece, :, :width] = gate.astype(BF16)
            up = jnp.dot(mixer_in, wu[:, columns], preferred_element_type=F32)
            d_send[piece, :, width : 2 * width] = up.astype(BF16)
            if j == 0:
                d_send[piece, :, 2 * width :] = square_tile
            copy = pltpu.make_async_remote_copy(
                src_ref=d_send.at[piece],
                dst_ref=d_recv.at[me],
                send_sem=piece_send.at[piece, j],
                recv_sem=kv_recv.at[6 + j, me],
                device_id={"kv": target},
                device_id_type=pl.DeviceIdType.MESH,
            )
            d_copies.append((target, copy))
            pl.when(me != target)(copy.start)

    e_phase = 6 + len(widths)

    @pl.when(reduces)
    def _():
        own = me - first
        row_squares = squares
        for j, (d_send, d_recv, e_all, width, _) in enumerate(grids):
            gate = d_send[own, :, :width].astype(F32)
            up = d_send[own, :, width : 2 * width].astype(F32)
            for peer in reversed(peers):
                from_kv(6 + j, d_recv.at[peer], peer)
                gate = gate + d_recv[peer, :, :width].astype(F32)
                up = up + d_recv[peer, :, width : 2 * width].astype(F32)
                if j == 0:
                    row_squares = row_squares + from_high_low(
                        d_recv[peer, :, 2 * width :]
                    )
            mixer_scale = lax.rsqrt(row_squares / features + EPSILON)
            gate = gate * mixer_scale
            up = up * mixer_scale
            e_all[own] = (gate / (1.0 + jnp.exp(-gate)) * up).astype(BF16)
            for i, peer in enumerate(peers):
                kv_copy(e_phase + j, e_all.at[own], e_all.at[own], i, own, peer).start()

    loads[12].wait()
    projected = jnp.zeros((rows, wd.shape[1]), F32)
    for j, (_, _, e_all, width, start) in enumerate(grids):
        for piece in [near] + ([far] if n_pieces > 1 else []):
            arrival = kv_copy(e_phase + j, e_all.at[piece], e_all.at[piece], 0, piece, me)
            pl.when(me != first + piece)(arrival.wait_recv)
            part = wd[pl.ds(pl.multiple_of(piece * span + start, LANES), width), :]
            projected = projected + jnp.dot(
                e_all[piece], part, preferred_element_type=F32
            )
    projected = projected.astype(BF16)
    f_send[...] = projected
    copies = [to_tp(1, k, f_send, f_recv.at[k - 1]) for k in range(1, n_tp)]
    mixed = projected.astype(F32)
    for k, copy in enumerate(copies):
        copy.wait_recv()
        mixed = mixed + f_recv[k].astype(F32)
    out_ref[...] = (mid_float + mixed).astype(BF16)
    for copy in pending:
        copy.wait_send()
    for target, copy in d_copies:
        pl.when(me != target)(copy.wait_send)

    @pl.when(reduces)
    def _():
        own = me - first
        for j, (_, _, e_all, _, _) in enumerate(grids):
            for i, peer in enumerate(peers):
                kv_copy(e_phase + j, e_all.at[own], e_all.at[own], i, own, peer).wait_send()


def rope_table(context):
    half = HD // 2
    frequency = (ROPE_BASE ** (-np.arange(half) * 2.0 / HD)).astype(np.float32)
    angles = (np.float32(context) * frequency).astype(np.float64)
    cosine = np.tile(np.cos(angles), LANES // half)
    sine = np.tile(np.concatenate([-np.sin(angles), np.sin(angles)]), LANES // HD)
    return np.stack([cosine, sine]).astype(np.float32)


def on_device(n_kv, n_tp, *arrays):
    (
        tokens,
        attend_gain,
        query_weight,
        cache_keys,
        cache_values,
        head_lambda,
        head_gain,
        output_weight,
        mixer_gain,
        gate_weight,
        up_weight,
        down_weight,
    ) = arrays
    rows, local = tokens.shape
    positions, kv_local = cache_keys.shape[1:3]
    heads = head_lambda.shape[0]
    assert kv_local == 1
    hidden = gate_weight.shape[1]
    n_pieces = min(2, n_kv)
    tiles = hidden // n_pieces // LANES
    assert tiles * n_pieces * LANES == hidden
    widths = [(tiles + 1) // 2 * LANES, tiles // 2 * LANES]
    count = rows * 2 * heads
    query_width = query_weight.shape[1]
    partners = max(n_tp - 1, 1)
    buffers = [2 * widths[0] + LANES, 2 * widths[1]]
    phases = 6 + 2 * len(widths)
    operands = (
        tokens,
        attend_gain.reshape(1, -1),
        query_weight,
        cache_keys.reshape(rows, positions, -1),
        cache_values.reshape(rows, positions, -1),
        head_lambda.reshape(1, -1),
        head_gain.reshape(1, -1),
        output_weight,
        mixer_gain.reshape(1, -1),
        gate_weight,
        up_weight,
        down_weight,
        jnp.asarray(rope_table(positions * n_kv)),
    )
    loaded = [pltpu.VMEM(a.shape, a.dtype) for a in operands]
    return pl.pallas_call(
        functools.partial(kernel, n_kv, n_tp, n_pieces, widths, local * n_kv),
        out_shape=jax.ShapeDtypeStruct(tokens.shape, tokens.dtype),
        in_specs=[pl.BlockSpec(memory_space=pl.ANY)] * len(operands),
        out_specs=pl.BlockSpec(memory_space=pltpu.VMEM),
        scratch_shapes=loaded
        + [
            pltpu.VMEM((rows, query_width + LANES), BF16),
            pltpu.VMEM((n_kv, rows, query_width + LANES), BF16),
            pltpu.VMEM((count, LANES), BF16),
            pltpu.VMEM((n_kv, count, LANES), BF16),
            pltpu.VMEM((2, count), F32),
            pltpu.VMEM((n_kv, 2, count), F32),
            pltpu.VMEM((rows, local), BF16),
            pltpu.VMEM((partners, rows, local), BF16),
            [pltpu.VMEM((n_pieces, rows, size), BF16) for size in buffers],
            [pltpu.VMEM((n_kv, rows, size), BF16) for size in buffers],
            [pltpu.VMEM((n_pieces, rows, size), BF16) for size in widths],
            pltpu.VMEM((rows, local), BF16),
            pltpu.VMEM((partners, rows, local), BF16),
            pltpu.VMEM((heads * rows, LANES), F32),
            pltpu.VMEM((heads * rows, LANES), F32),
            pltpu.SemaphoreType.DMA((len(operands),)),
            pltpu.SemaphoreType.DMA((phases, n_kv)),
            pltpu.SemaphoreType.DMA((phases, n_kv)),
            pltpu.SemaphoreType.DMA((n_pieces, len(widths))),
            pltpu.SemaphoreType.DMA((2, partners)),
            pltpu.SemaphoreType.DMA((2, partners)),
        ],
        compiler_params=pltpu.CompilerParams(
            collective_id=0, has_side_effects=True
        ),
    )(*operands)


def solution(mesh):
    return jax.shard_map(
        functools.partial(on_device, mesh.shape["kv"], mesh.shape["tp"]),
        mesh=mesh,
        in_specs=(
            P(("grp", "dp"), "kv"),
            P("kv"),
            P("kv", "tp"),
            P(("grp", "dp"), "kv", "tp", None),
            P(("grp", "dp"), "kv", "tp", None),
            P("tp"),
            P(),
            P("tp", "kv"),
            P("kv"),
            P("kv", "tp"),
            P("kv", "tp"),
            P("tp", "kv"),
        ),
        out_specs=P(("grp", "dp"), "kv"),
        check_vma=False,
    )
```

time: 132 us -> 26.7 us (0.20)
  blocking collectives: 65.5 us -> 0 us
  waiting for transfers between devices: 32.8 us -> 0 us
  Pallas kernels: 0 us -> 25.2 us
  between operations: 13.5 us -> 0.01 us
  matrix products: 10.6 us -> 0 us
  other arithmetic: 4.88 us -> 0 us
  local copies, waits for them, and re-layouts: 3.83 us -> 1.3 us
    all_gather x3 -> x0, blocking collectives: 39.8 us -> none  [merged(): lax.all_gather(a.astype(kind), axis)]
    psum x1 -> x0, waiting for transfers between devices: 32.8 us -> none  [on_device(): lax.psum(up_part.astype(jnp.bfloat16), 'kv').astype(jnp.float32)]
    psum x3 -> x0, blocking collectives: 25.6 us -> none  [the longest x1 20.7 us: on_device(): lax.psum(partial_query.astype(jnp.bfloat16), 'kv').astype(jnp.float32)]
    pallas_call x0 -> x1, Pallas kernels: none -> 25.2 us  [on_device(): pl.pallas_call(functools.partial(kernel, n_kv, n_tp, n_pieces, widths, lo...]
    dot_general x7 -> x0, matrix products: 10.6 us -> none  [the longest x1 2.4 us: on_device(): projected = jnp.dot(hidden, down_weight, preferred_element_type=jnp.float32)]
    reduce_sum x4 -> x0, other arithmetic: 1.95 us -> none  [the longest x1 0.97 us: on_device(): jnp.sum(tok_float * tok_float, axis=1).astype(jnp.bfloat16)]
  transfers between devices with their start and end apart: 1 -> 0, of which waited for: 1 -> 0; matrix products, arithmetic and copies ran while one was open for 0% -> 0% of each run, Pallas kernels for 0% -> 0%
where the time goes in v1:
time: 26.7 us; the launch traced here: 26.5 us
  Pallas kernels  25.2 us (94%)
  local copies, waits for them, and re-layouts  1.3 us (5%)
    pallas_call x1, Pallas kernels, on_device(): pl.pallas_call(functools.partial(kernel, n_kv, n_tp, n_pieces, widths, lo...  25.2 us
    unnamed x1, local copies, waits for them, and re-layouts  1.3 us

profile of v1, /device:TPU:0, one launch (start us, length us, event | category | flops | bytes accessed | tf_op | source)
XLA Modules:
  0.0 26.5 jit_solution(7465868540805149278)
XLA Ops:
  0.0 25.2 %shard_map.127 = bf16[8,512]{1,0:T(8,128)(2,1)} custom-call(bf16[8,512]{1,0:T(8,128)(2,1)} %tok_hbm.1, f32[1,512]{1,0:T(1,128)} %bitcast.8, bf16[512,1024]{1,0:T(8,128)(2,1)} %wq_hbm.1, bf16[8,384,128]{2,1,0:T(8,128)(2,1)} %bitcast.6, bf16[8,384,128]{2,1,0:T(8,128)(2,1)} %bitcast.7, f32[1,8]{1,0:T(1,128)} %bitcast.10, f32[1,128]{1,0:T(1,128)} %bitcast.11, ...), custom_call_target="tpu_custom_call" | custom-call | tf_op jit(solution)/shard_map/pallas_call | solution.py:439
  25.2 1.3 %copy.15 = bf16[8,512]{1,0:T(8,128)(2,1)} copy(bf16[8,512]{1,0:T(8,128)(2,1)} %shard_map.127) | data formatting | bytes 16384

commit v2 on v1

--- a/solution.py
+++ b/solution.py
@@ -13,7 +13,7 @@
 EPSILON = 1e-06
 KEEP_SCALE = 0.8
 LANES = 128
-B_PARTS = 2
+B_PARTS = 4
 F32 = jnp.float32
 BF16 = jnp.bfloat16
 
@@ -438,7 +438,7 @@
     loaded = [pltpu.VMEM(a.shape, a.dtype) for a in operands]
     return pl.pallas_call(
         functools.partial(kernel, n_kv, n_tp, n_pieces, widths, local * n_kv),
-        out_shape=jax.ShapeDtypeStruct(tokens.shape, tokens.dtype),
+        out_shape=pltpu.VMEM(tokens.shape, tokens.dtype),
         in_specs=[pl.BlockSpec(memory_space=pl.ANY)] * len(operands),
         out_specs=pl.BlockSpec(memory_space=pltpu.VMEM),
         scratch_shapes=loaded

time: 26.7 us -> 25.3 us (0.948)
  local copies, waits for them, and re-layouts: 1.3 us -> 0.6 us
  Pallas kernels: 25.2 us -> 24.5 us
    unnamed x1, local copies, waits for them, and re-layouts: 1.3 us -> 0.6 us
    pallas_call x1, Pallas kernels: 25.2 us -> 24.5 us  [on_device(): pl.pallas_call(functools.partial(kernel, n_kv, n_tp, n_pieces, widths, lo...]
where the time goes in v2:
time: 25.3 us; the launch traced here: 25.1 us
  Pallas kernels  24.5 us (97%)
  local copies, waits for them, and re-layouts  0.6 us (2%)
    pallas_call x1, Pallas kernels, on_device(): pl.pallas_call(functools.partial(kernel, n_kv, n_tp, n_pieces, widths, lo...  24.5 us
    unnamed x1, local copies, waits for them, and re-layouts  0.6 us

profile of v2, /device:TPU:0, one launch (start us, length us, event | category | flops | bytes accessed | tf_op | source)
XLA Modules:
  0.0 25.1 jit_solution(10137788671532727578)
XLA Ops:
  0.0 24.5 %shard_map.127 = bf16[8,512]{1,0:T(8,128)(2,1)S(1)} custom-call(bf16[8,512]{1,0:T(8,128)(2,1)} %tok_hbm.1, f32[1,512]{1,0:T(1,128)} %bitcast.8, bf16[512,1024]{1,0:T(8,128)(2,1)} %wq_hbm.1, bf16[8,384,128]{2,1,0:T(8,128)(2,1)} %bitcast.6, bf16[8,384,128]{2,1,0:T(8,128)(2,1)} %bitcast.7, f32[1,8]{1,0:T(1,128)} %bitcast.10, f32[1,128]{1,0:T(1,128)} %bitcast.11, ...), custom_call_target="tpu_custom_call" | custom-call | tf_op jit(solution)/shard_map/pallas_call | solution.py:439
  24.5 0.6 %copy.15 = bf16[8,512]{1,0:T(8,128)(2,1)} copy(bf16[8,512]{1,0:T(8,128)(2,1)S(1)} %shard_map.127) | data formatting | bytes 16384
